TPU v7x, 128 devices: a whole 4x4x4 slice. The times are simulated.
128 devices in a mesh: sp: 16 (over z, y), tp: 8 (over x, core).
Axes of the slice: x: 4, y: 4, z: 4, core: 2. Of those that a mesh axis runs over, the one named last changes fastest.
Arguments:
- query_proj: bfloat16 [16384, 2048], P('sp', 'tp'), may hold values from -6 to 6
- key_proj: bfloat16 [16384, 2048], P('sp', 'tp'), may hold values from -6 to 6
- value_proj: bfloat16 [16384, 4096], P('sp', 'tp'), may hold values from -6 to 6
- gate_proj: bfloat16 [16384, 4096], P('sp', 'tp'), may hold values from -6 to 6
- log_decay: float32 [16384, 8], P('sp', 'tp'), may hold values from -0.75 to 0, as said below
- residual: bfloat16 [16384, 2048], P('sp'), may hold values from -4 to 4
- out_weight: bfloat16 [4096, 2048], P('tp'), may hold values from -0.09375 to 0.09375
- norm_gain: float32 [2, 2048], replicated, may hold values from 0.1 to 1.9
- norm_bias: float32 [2, 2048], replicated, may hold values from -1.5 to 1.5
- up_gate: bfloat16 [2048, 5632], P('sp', 'tp'), may hold values from -0.125 to 0.125
- up_value: bfloat16 [2048, 5632], P('sp', 'tp'), may hold values from -0.125 to 0.125
- conv_weight: float32 [2, 3, 5632], P(None, None, 'tp'), may hold values from -3 to 3
- conv_bias: float32 [2, 5632], P(None, 'tp'), may hold values from -1.5 to 1.5
- down_weight: bfloat16 [5632, 2048], P('tp', 'sp'), may hold values from -0.078125 to 0.078125
Outputs:
- layer_output: bfloat16 [16384, 2048], P(('sp', 'tp'))
Inputs may be any that keep to these rules, and one draw needn't show every extreme that they name: `log_decay`: all entries are negative.
All inputs are finite; a program needn't handle non-finite values.
Results may differ from a plain program's by a relative error of at most 0.023.
Values may be sent and summed in bfloat16 or wider, within the bound.
No kernel may reach another device: no remote copies, remote signals or barrier semaphores. Data moves between devices by JAX's collectives and lax.ppermute only.
A program may use at most 128 MiB of HBM per device.

v0:
```python
import jax
import jax.numpy as jnp
from jax import lax
from jax.sharding import Mesh
from jax.sharding import PartitionSpec as P

BLOCK = 256
SP = ("sp_0", "sp_1")
SP_TP = ("sp_0", "sp_1", "tp")
alpha_scale = 8.0**0.25
rope_base = 10000.0
tiny_stabilizer = 1e-05


def turned_gather(arrays, axis, dims):
    turned = [jnp.moveaxis(a, dim, 0) for a, dim in zip(arrays, dims)]
    both = jnp.concatenate([t.reshape(len(t), -1) for t in turned], axis=1)
    out, at, finished = (lax.all_gather(both, axis, axis=0, tiled=True), 0, [])
    for t, dim in zip(turned, dims):
        piece = out[:, at : at + t[0].size].reshape(-1, *t.shape[1:])
        finished.append(jnp.moveaxis(piece, 0, dim))
        at += t[0].size
    return tuple(finished)


def neutral_like(x, identity):
    return jax.tree.map(
        lambda a, e: jnp.broadcast_to(jnp.asarray(e, a.dtype), a.shape), x, identity
    )


def entering(x, axes, combine, identity):
    before = start = neutral_like(x, identity)
    subtotal = x
    for axis in reversed(axes):
        length, position = (lax.axis_size(axis), lax.axis_index(axis))
        pieces = jax.tree.map(
            lambda part, kind: lax.all_gather(part.astype(kind), axis),
            subtotal,
            (jnp.bfloat16, jnp.bfloat16),
        )
        inside, subtotal = (start, start)
        for k in range(length):
            passed = k < position
            subtotal = combine(
                subtotal, jax.tree.map(lambda part, own: part[k].astype(own.dtype), pieces, x)
            )
            inside = jax.tree.map(lambda new, old: jnp.where(passed, new, old), subtotal, inside)
        before = combine(inside, before)
    return before


def passed_along(x, axis, by):
    length = lax.axis_size(axis)
    pairs = [(i, i + by) for i in range(length) if 0 <= i + by < length]
    return lax.ppermute(x, axis, pairs)


def rotate(vectors, positions):
    head_width = vectors.shape[-1]
    half_width = head_width // 2
    inverse_freq = rope_base ** (-2.0 * jnp.arange(half_width, dtype=jnp.float32) / head_width)
    angles = positions[:, None] * inverse_freq[None, :]
    cosine = jnp.cos(angles)[:, None, :]
    sine_part = jnp.sin(angles)[:, None, :]
    front = vectors[..., :half_width]
    second = vectors[..., half_width:]
    return jnp.concatenate(
        [front * cosine - second * sine_part, front * sine_part + second * cosine], axis=-1
    )


def layer_norm(values, gain, shift):
    average = values.mean(-1, keepdims=True)
    spread = jnp.square(values - average).mean(-1, keepdims=True)
    return (values - average) * lax.rsqrt(spread + tiny_stabilizer) * gain + shift


def block_parts(query_tile, lookup_piece, payload_piece, log_blk):
    cum_log = jnp.cumsum(log_blk, axis=0)
    cum_heads = cum_log.T
    log_gap = cum_heads[:, :, None] - cum_heads[:, None, :]
    offsets = jnp.arange(log_blk.shape[0])
    causal = (offsets[:, None] >= offsets[None, :])[None]
    weight = jnp.where(causal, jnp.exp(jnp.where(causal, log_gap, 0.0)), 0.0)
    score_matrix = jnp.einsum(
        "jka,ska->kjs", query_tile, lookup_piece, preferred_element_type=jnp.float32
    )
    segment_scaling = (score_matrix * weight).astype(jnp.bfloat16)
    within = jnp.einsum(
        "htm,mhe->the", segment_scaling, payload_piece, preferred_element_type=jnp.float32
    )
    block_total = cum_log[-1]
    to_end = jnp.exp(block_total[None, :] - cum_log)
    faded_lookup_vector = (lookup_piece.astype(jnp.float32) * to_end[:, :, None]).astype(
        jnp.bfloat16
    )
    summand_term = jnp.einsum(
        "ajo,ajd->jod", faded_lookup_vector, payload_piece, preferred_element_type=jnp.float32
    )
    scaled_query = (query_tile.astype(jnp.float32) * jnp.exp(cum_log)[:, :, None]).astype(
        jnp.bfloat16
    )
    return (within, scaled_query, summand_term, jnp.exp(block_total))


def causal_conv(rows, edge_rows, taps, shift):
    padded = jnp.concatenate([edge_rows, rows], axis=0).astype(jnp.float32)
    length = rows.shape[0]
    result = shift[None, :] + padded[0:length] * taps[0]
    result = result + padded[1 : length + 1] * taps[1]
    return result + padded[2 : length + 2] * taps[2]


def combine(earlier, later):
    return (earlier[0] * later[0], later[0][:, None, None] * earlier[1] + later[1])


def shards(
    query_proj,
    key_proj,
    value_proj,
    gate_proj,
    log_decay,
    residual,
    out_weight,
    norm_gain,
    norm_bias,
    up_gate,
    up_value,
    conv_weight,
    conv_bias,
    down_weight,
):
    tok_rows = query_proj.shape[0]
    head_count = log_decay.shape[1]
    key_width = query_proj.shape[1] // head_count
    value_width = value_proj.shape[1] // head_count
    full_gate, full_value, full_down = turned_gather(
        (up_gate, up_value, down_weight), SP, (0, 0, 1)
    )
    positions = (lax.axis_index(SP) * tok_rows + jnp.arange(tok_rows)).astype(jnp.float32)
    query_rot = rotate(
        query_proj.astype(jnp.float32).reshape(tok_rows, head_count, key_width), positions
    ).astype(jnp.bfloat16)
    key_rot = (
        rotate(key_proj.astype(jnp.float32).reshape(tok_rows, head_count, key_width), positions)
        * key_width ** (-0.5)
    ).astype(jnp.bfloat16)
    block_count = tok_rows // BLOCK
    asking_segments = query_rot.reshape(block_count, BLOCK, head_count, key_width)
    key_blocks = key_rot.reshape(block_count, BLOCK, head_count, key_width)
    value_blocks = value_proj.reshape(block_count, BLOCK, head_count, value_width)
    log_blocks = log_decay.reshape(block_count, BLOCK, head_count)
    within, scaled_query, summand_term, block_decay = jax.vmap(block_parts)(
        asking_segments, key_blocks, value_blocks, log_blocks
    )

    def absorb(carry_state, pieces):
        return (pieces[1][:, None, None] * carry_state + pieces[0], None)

    zero_state = jnp.zeros((head_count, key_width, value_width), jnp.float32)
    own_state, _ = lax.scan(absorb, zero_state, (summand_term, block_decay))
    own_decay = jnp.prod(block_decay, axis=0)
    _, incoming = entering(
        (own_decay, own_state), SP, combine, (jnp.ones_like(own_decay), zero_state)
    )

    def advance(carry_state, pieces):
        carried = jnp.einsum(
            "thd,hde->the",
            pieces[0],
            carry_state.astype(jnp.bfloat16),
            preferred_element_type=jnp.float32,
        )
        return (pieces[2][:, None, None] * carry_state + pieces[1], carried)

    _, carried = lax.scan(advance, incoming, (scaled_query, summand_term, block_decay))
    mixed_heads = (within + carried).reshape(tok_rows, head_count, value_width)
    average = mixed_heads.mean(-1, keepdims=True)
    spread = jnp.square(mixed_heads - average).mean(-1, keepdims=True)
    standardized_rows = (mixed_heads - average) * lax.rsqrt(spread + tiny_stabilizer)
    gate_heads = gate_proj.astype(jnp.float32).reshape(tok_rows, head_count, value_width)
    gated_rows = (
        (jax.nn.silu(gate_heads) * standardized_rows)
        .astype(jnp.bfloat16)
        .reshape(tok_rows, head_count * value_width)
    )
    own_count = tok_rows // lax.axis_size("tp")
    partial_rows = jnp.dot(gated_rows, out_weight, preferred_element_type=jnp.float32)
    attended = lax.psum_scatter(
        partial_rows.astype(jnp.bfloat16), "tp", scatter_dimension=0, tiled=True
    ).astype(jnp.float32)
    own_residual = lax.dynamic_slice_in_dim(
        residual, lax.axis_index("tp") * own_count, own_count, 0
    )
    normed_own = layer_norm(
        alpha_scale * own_residual.astype(jnp.float32) + attended, norm_gain[0], norm_bias[0]
    ).astype(jnp.bfloat16)
    whole_rows = lax.all_gather(normed_own, "tp", axis=0, tiled=True)
    gate_up = jnp.dot(whole_rows, full_gate, preferred_element_type=jnp.float32)
    value_up = jnp.dot(whole_rows, full_value, preferred_element_type=jnp.float32)
    gate_up = gate_up.astype(jnp.bfloat16)
    value_up = value_up.astype(jnp.bfloat16)
    edges = jnp.concatenate([gate_up[tok_rows - 2 :], value_up[tok_rows - 2 :]], axis=0)
    edges = passed_along(edges, SP, 1)
    gate_edge, value_edge = (edges[:2], edges[2:])
    gate_conv = causal_conv(gate_up, gate_edge, conv_weight[0], conv_bias[0])
    value_conv = causal_conv(value_up, value_edge, conv_weight[1], conv_bias[1])
    activated = (jax.nn.gelu(gate_conv) * value_conv).astype(jnp.bfloat16)
    partial_ffn = jnp.dot(activated, full_down, preferred_element_type=jnp.float32)
    ffn_out = lax.psum_scatter(
        partial_ffn.astype(jnp.bfloat16), "tp", scatter_dimension=0, tiled=True
    ).astype(jnp.float32)
    return layer_norm(
        alpha_scale * normed_own.astype(jnp.float32) + ffn_out, norm_gain[1], norm_bias[1]
    ).astype(jnp.bfloat16)


def solution(mesh):
    torus = Mesh(mesh.devices.reshape(4, 4, mesh.shape["tp"]), ("sp_0", "sp_1", "tp"))
    return jax.shard_map(
        shards,
        mesh=torus,
        in_specs=(
            P(SP, "tp"),
            P(SP, "tp"),
            P(SP, "tp"),
            P(SP, "tp"),
            P(SP, "tp"),
            P(SP, None),
            P("tp", None),
            P(),
            P(),
            P(SP, "tp"),
            P(SP, "tp"),
            P(None, None, "tp"),
            P(None, "tp"),
            P("tp", SP),
        ),
        out_specs=P(SP_TP, None),
        check_vma=False,
    )
```

profile of v0, /device:TPU:0, one launch (start us, length us, event | category | flops | bytes accessed | tf_op | source)
XLA Modules:
  0.0 314.5 jit_solution(11302256274251141249)
XLA Ops:
  7.4 2.4 reduce-window.6
  10.4 1.4 bitcast_convert_fusion
  11.8 3.1 fusion.56
  15.7 2.0 convolution_bitcast_fusion.1
  17.7 9.8 %while.24 = (s32[]{:T(128)}, f32[1,256,512]{2,1,0:T(8,128)S(1)}, f32[4,1]{0,1:T(1,128)S(1)}, f32[4,1,256,512]{3,2,1,0:T(8,128)}, s32[]{:T(128)}, /*index=5*/s32[]{:T(128)}) while((s32[]{:T(128)}, f32[1,256,512]{2,1,0:T(8,128)S(1)}, f32[4,1]{0,1:T(1,128)S(1)}, f32[4,1,256,512]{3,2,1,0:T(8,128)}, s32[]{:T(128)}, ...), condition=%wide.region_4.5_spmd.clone, body=%wide.region_3.4_spmd.clone.sunk | while | flops 393219 | bytes 1572971 | solution.py:163
  18.3 1.8 bitcast_add_fusion.8
  20.8 1.8 bitcast_add_fusion.8
  23.2 1.8 bitcast_add_fusion.8
  25.7 1.8 bitcast_add_fusion.8
  29.7 1.4 dynamic-update-slice
  31.0 10.8 %all-reduce = bf16[4]{0:T(256)(128)(2,1)S(1)} all-reduce(bf16[4]{0:T(256)(128)(2,1)S(1)} %dynamic-update-slice), channel_id=1, replica_groups=mesh['sp_0'=4,'sp_1'=4,'tp'=8] {'sp_1'}, use_global_device_ids=true, to_apply=%add | all-reduce | flops 4 | bytes 16
  43.2 11.9 %all-gather.13.cloned.1.call-done = bf16[4,256,512]{2,1,0:T(8,128)(2,1)} async-done(((bf16[1,256,512]{2,1,0:T(8,128)(2,1)}), bf16[4,256,512]{2,1,0:T(8,128)(2,1)}) %all-gather.13.cloned.1.call-update) | async-done | bytes 1048592 | tf_op jit(solution)/shard_map/all_gather | solution.py:38
  55.0 4.0 %fusion.70 = bf16[1,1,256,512]{3,2,1,0:T(8,128)(2,1)} fusion(f32[]{:T(128)} %bitcast.39, f32[]{:T(128)} %bitcast.40, f32[]{:T(128)} %bitcast.41, f32[]{:T(128)} %bitcast.42, bf16[4,256,512]{2,1,0:T(8,128)(2,1)} %all-gather.13.cloned.1.call-done), kind=kLoop, calls=%fused_computation.102 | loop fusion | flops 1572864 | bytes 1310736 | tf_op jit(solution)/shard_map/convert_element_type | solution.py:38
  60.4 1.4 dynamic-update-slice.1
  61.8 10.7 %all-reduce.1 = bf16[4]{0:T(256)(128)(2,1)S(1)} all-reduce(bf16[4]{0:T(256)(128)(2,1)S(1)} %dynamic-update-slice.1), channel_id=2, replica_groups=mesh['sp_0'=4,'sp_1'=4,'tp'=8] {'sp_0'}, use_global_device_ids=true, to_apply=%add.1 | all-reduce | flops 4 | bytes 16
  78.2 1.9 fusion.61
  80.2 3.6 %all-gather.7.cloned.1.call-done = bf16[4,1,256,512]{3,2,1,0:T(8,128)(2,1)} async-done(((bf16[1,1,256,512]{3,2,1,0:T(8,128)(2,1)}), bf16[4,1,256,512]{3,2,1,0:T(8,128)(2,1)}) %all-gather.7.cloned.1.call-update) | async-done | bytes 1048592 | tf_op jit(solution)/shard_map/all_gather | solution.py:38
  83.8 3.9 %fusion.69 = f32[1,256,512]{2,1,0:T(8,128)S(1)} fusion(bf16[4,1,256,512]{3,2,1,0:T(8,128)(2,1)} %all-gather.7.cloned.1.call-done, f32[]{:T(128)} %bitcast.39, f32[]{:T(128)} %bitcast.40, f32[]{:T(128)} %bitcast.41, f32[]{:T(128)} %bitcast.42, f32[]{:T(128)} %bitcast.33, f32[]{:T(128)S(6)} %convert.26, f32[]{:T(128)S(6)} %convert.27, f32[]{:T(128)} %bitcast.38, ...), kind=kLoop, calls=%fused_computation.99 | loop fusion | flops 4194304 | bytes 2621484 | tf_op jit(solution)/shard_map/add | solution.py:116
  87.7 17.8 %while.23 = (s32[]{:T(128)}, f32[1,256,512]{2,1,0:T(8,128)S(1)}, f32[4,256,1,512]{3,1,2,0:T(8,128)}, f32[4,1]{0,1:T(1,128)S(1)}, f32[4,1,256,512]{3,2,1,0:T(8,128)}, /*index=5*/bf16[4,256,1,256]{3,1,2,0:T(8,128)(2,1)}, s32[]{:T(128)}) while((s32[]{:T(128)}, f32[1,256,512]{2,1,0:T(8,128)S(1)}, f32[4,256,1,512]{3,1,2,0:T(8,128)}, ...), condition=%wide.region_6.7_spmd, body=%wide.region_5.6_spmd.sunk | while | flops 67502080 | bytes 2753641 | solution.py:178
  88.4 1.9 fusion.118
  90.3 1.9 bitcast_add_fusion.7
  92.8 1.9 fusion.118
  94.7 1.9 bitcast_add_fusion.7
  97.2 1.9 fusion.118
  99.2 1.9 bitcast_add_fusion.7
  101.7 1.9 fusion.118
  103.6 1.9 bitcast_add_fusion.7
  105.5 4.2 %fusion.102 = (f32[4,256]{1,0:T(4,128)S(1)}, f32[4,256,1,512]{3,1,0,2:T(8,128)}) fusion(f32[4,256,1,512]{3,1,2,0:T(8,128)} %get-tuple-element.60, bf16[4,256,512]{2,1,0:T(8,128)(2,1)} %bitcast.150, bf16[4,256,128]{2,1,0:T(8,128)(2,1)} %bitcast.155, bf16[4,256,128]{2,1,0:T(8,128)(2,1)S(1)} %bitcast.153, f32[4,256]{1,0:T(4,128)S(1)} %get-tuple-element.145, ...), kind=kOutput, calls=%fused_computation.160 | convolution fusion | flops 406846464 | bytes 6889472 | tf_op jit(solution)/shard_map/vmap(htm,mhe->the)/dot_general | solution.py:90
  109.8 2.1 multiply_reduce_fusion
  112.0 2.2 fusion.31
  114.2 4.3 %convolution_convert_fusion.1 = bf16[1024,2048]{1,0:T(8,128)(2,1)} fusion(bf16[1024,512]{1,0:T(8,128)(2,1)S(1)} %fusion.31, bf16[512,2048]{1,0:T(8,128)(2,1)S(1)} %copy-done), kind=kOutput, calls=%fused_computation.14 | convolution fusion | flops 2149580800 | bytes 7340032 | tf_op jit(solution)/shard_map/dot_general | solution.py:190
  118.6 0.8 copy-done.5
  119.6 0.9 pad_maximum_fusion
  120.6 36.8 %reduce-scatter.3.cloned.1.call-done = bf16[128,2048]{1,0:T(8,128)(2,1)} async-done(((bf16[1024,2048]{1,0:T(8,128)(2,1)}), bf16[128,2048]{1,0:T(8,128)(2,1)}) %reduce-scatter.3.cloned.1.call-update) | async-done | bytes 524304 | tf_op jit(solution)/shard_map/reduce_scatter | solution.py:191
  157.4 1.5 fusion.45
  158.9 1.6 multiply_reduce_fusion.2
  160.4 2.4 add_convert_fusion.1
  163.1 36.6 %all-gather.11.cloned.1.call-done = bf16[2048,2112]{0,1:T(8,128)(2,1)} async-done(((bf16[128,2112]{0,1:T(8,128)(2,1)}), bf16[2048,2112]{0,1:T(8,128)(2,1)}) %all-gather.11.cloned.1.call-update) | async-done | bytes 8650768 | tf_op jit(solution)/shard_map/all_gather | solution.py:18
  199.7 32.7 %all-gather.9.cloned.1.call-done = bf16[1024,2048]{1,0:T(8,128)(2,1)} async-done(((bf16[128,2048]{1,0:T(8,128)(2,1)}), bf16[1024,2048]{1,0:T(8,128)(2,1)}) %all-gather.9.cloned.1.call-update) | async-done | bytes 4194320 | tf_op jit(solution)/shard_map/all_gather | solution.py:200
  232.4 6.4 %fusion.32 = bf16[1024,704]{0,1:T(8,128)(2,1)S(1)} fusion(bf16[1024,2048]{1,0:T(8,128)(2,1)} %all-gather.9.cloned.1.call-done, bf16[2048,2112]{0,1:T(8,128)(2,1)} %all-gather.11.cloned.1.call-done), kind=kOutput, calls=%fused_computation.52 | convolution fusion | flops 2953510912 | bytes 8519680 | tf_op jit(solution)/shard_map/dot_general | solution.py:201
  239.0 5.0 %fusion.35 = bf16[1024,704]{0,1:T(8,128)(2,1)S(1)} fusion(bf16[1024,2048]{1,0:T(8,128)(2,1)S(1)} %copy-done.12, bf16[2048,2112]{0,1:T(8,128)(2,1)} %all-gather.11.cloned.1.call-done), kind=kOutput, calls=%fused_computation.53 | convolution fusion | flops 2953510912 | bytes 8519680 | tf_op jit(solution)/shard_map/dot_general | solution.py:202
  244.3 3.6 %collective-permute-start = (bf16[4,704]{0,1:T(8,128)(2,1)S(1)}, bf16[4,704]{0,1:T(8,128)(2,1)S(1)}, u32[]{:S(2)}, u32[]{:S(2)}) collective-permute-start(bf16[4,704]{0,1:T(8,128)(2,1)S(1)} %pad_maximum_fusion.1), channel_id=1, source_target_pairs={{0,8},{8,16},{16,24},{24,32},{32,40},{40,48},{48,56},{56,64},{64,7... | collective-permute-start | bytes 16904 | tf_op jit(solution)/shard_map/ppermute | solution.py:56
  247.9 3.9 %collective-permute-done = bf16[4,704]{0,1:T(8,128)(2,1)S(1)} collective-permute-done((bf16[4,704]{0,1:T(8,128)(2,1)S(1)}, bf16[4,704]{0,1:T(8,128)(2,1)S(1)}, u32[]{:S(2)}, u32[]{:S(2)}) %collective-permute-start) | collective-permute-done | bytes 5664 | tf_op jit(solution)/shard_map/ppermute | solution.py:56
  253.5 10.0 %convolution_convert_fusion = bf16[1024,2048]{1,0:T(8,128)(2,1)} fusion(bf16[2048,2112]{0,1:T(8,128)(2,1)} %all-gather.11.cloned.1.call-done, f32[1026,704]{0,1:T(8,128)S(1)} %maximum_convert_fusion.1, f32[1026,704]{0,1:T(8,128)S(1)} %maximum_convert_fusion, f32[704]{0:T(1024)S(1)} %get-tuple-element.120, f32[704]{0:T(1024)S(1)} %get-tuple-element.121, ...), kind=kOutput, calls=%fused_computation.13 | convolution fusion | flops 2970746880 | bytes 24412160 | tf_op jit(solution)/shard_map/dot_general | solution.py:211
  263.6 38.9 %reduce-scatter.5.cloned.1.call-done = bf16[128,2048]{1,0:T(8,128)(2,1)} async-done(((bf16[1024,2048]{1,0:T(8,128)(2,1)}), bf16[128,2048]{1,0:T(8,128)(2,1)}) %reduce-scatter.5.cloned.1.call-update) | async-done | bytes 524304 | tf_op jit(solution)/shard_map/reduce_scatter | solution.py:212
  302.5 1.3 fusion.46
  303.8 1.4 multiply_reduce_fusion.1
  305.2 2.2 add_convert_fusion
  (91 shorter events, 13.9 us)
Async XLA Ops:
  7.4 106.8 %copy-start = (bf16[512,2048]{1,0:T(8,128)(2,1)S(1)}, bf16[512,2048]{1,0:T(8,128)(2,1)}, u32[]{:S(2)}) copy-start(bf16[512,2048]{1,0:T(8,128)(2,1)} %param.24) | copy-start | bytes 6291460
  7.4 47.7 %all-gather.13.cloned.1.call-start = ((), (), s32[]{:S(2)}) async-start(), calls=%async_computation.7 | async-start | bytes 1310720 | tf_op jit(solution)/shard_map/all_gather | solution.py:38
  10.4 5.3 %copy-start.4 = (bf16[1024,512]{1,0:T(8,128)(2,1)S(1)}, bf16[1024,512]{1,0:T(8,128)(2,1)}, u32[]{:S(2)}) copy-start(bf16[1024,512]{1,0:T(8,128)(2,1)} %param.20) | copy-start | bytes 3145732
  14.9 0.8 copy-start.3
  17.7 10.6 %copy-start.14 = (u32[128]{0:T(128)S(1)}, u32[128]{0:T(128)}, u32[]{:S(2)}) copy-start(u32[128]{0:T(128)} %constant.99) | copy-start | bytes 1540
  17.7 41.3 %copy-start.13 = (u32[128]{0:T(128)S(1)}, u32[128]{0:T(128)}, u32[]{:S(2)}) copy-start(u32[128]{0:T(128)} %constant.104) | copy-start | bytes 1540
  28.3 55.6 %all-gather.7.cloned.1.call-start = ((), (), s32[]{:S(2)}) async-start(), calls=%async_computation.2 | async-start | bytes 1310720 | tf_op jit(solution)/shard_map/all_gather | solution.py:38
  59.0 98.4 %reduce-scatter.3.cloned.1.call-start = ((), (), s32[]{:S(2)}) async-start(), calls=%async_computation.3 | async-start | bytes 4718592 | tf_op jit(solution)/shard_map/reduce_scatter | solution.py:191
  109.7 2.2 copy-start.1
  118.5 0.9 copy-start.5
  118.5 1.0 copy-start.6
  118.5 1.1 copy-start.7
  118.5 2.1 copy-start.9
  118.5 2.1 copy-start.10
  118.5 81.2 %all-gather.11.cloned.1.call-start = ((), (), s32[]{:S(2)}) async-start(), calls=%async_computation.5 | async-start | bytes 9191424 | tf_op jit(solution)/shard_map/all_gather | solution.py:18
  119.6 43.5 %copy-start.8 = (f32[2,3,704]{2,0,1:T(2,128)S(1)}, f32[2,3,704]{2,0,1:T(2,128)}, u32[]{:S(2)}) copy-start(f32[2,3,704]{2,0,1:T(2,128)} %param.29) | copy-start | bytes 50692
  120.5 111.9 %all-gather.9.cloned.1.call-start = ((), (), s32[]{:S(2)}) async-start(), calls=%async_computation.4 | async-start | bytes 4718592 | tf_op jit(solution)/shard_map/all_gather | solution.py:200
  162.8 139.7 %reduce-scatter.5.cloned.1.call-start = ((), (), s32[]{:S(2)}) async-start(), calls=%async_computation.6 | async-start | bytes 4718592 | tf_op jit(solution)/shard_map/reduce_scatter | solution.py:212
  232.4 6.5 %copy-start.12 = (bf16[1024,2048]{1,0:T(8,128)(2,1)S(1)}, bf16[1024,2048]{1,0:T(8,128)(2,1)}, u32[]{:S(2)}) copy-start(bf16[1024,2048]{1,0:T(8,128)(2,1)} %all-gather.9.cloned.1.call-done) | copy-start | bytes 12582916
  239.0 8.9 %copy-start.11 = (f32[2,704]{1,0:T(2,128)S(1)}, f32[2,704]{1,0:T(2,128)}, u32[]{:S(2)}) copy-start(f32[2,704]{1,0:T(2,128)} %param.30) | copy-start | bytes 16900
  244.3 7.6 %collective-permute-start = (bf16[4,704]{0,1:T(8,128)(2,1)S(1)}, bf16[4,704]{0,1:T(8,128)(2,1)S(1)}, u32[]{:S(2)}, u32[]{:S(2)}) collective-permute-start(bf16[4,704]{0,1:T(8,128)(2,1)S(1)} %pad_maximum_fusion.1), channel_id=1, source_target_pairs={{0,8},{8,16},{16,24},{24,32},{32,40},{40,48},{48,56},{56,64},{64,7... | collective-permute-start | bytes 16904 | tf_op jit(solution)/shard_map/ppermute | solution.py:56
  263.5 39.0 %copy-start.2 = (bf16[128,2048]{1,0:T(8,128)(2,1)S(1)}, bf16[128,2048]{1,0:T(8,128)(2,1)}, u32[]{:S(2)}) copy-start(bf16[128,2048]{1,0:T(8,128)(2,1)} %add_convert_fusion.1) | copy-start | bytes 1572868
Sparse Core Ops, SparseCore 0:
  28.4 26.5 all-gather.12
  59.1 24.6 all-gather.6
  118.7 38.6 reduce-scatter.2
  263.7 38.7 reduce-scatter.4
Sparse Core Ops, SparseCore 1:
  121.1 78.5 all-gather.10
  201.3 31.1 all-gather.8
where the time goes:
time: 316 us; the launch traced here: 314 us
  waiting for transfers between devices  165 us (52%)
  other arithmetic  51.6 us (16%)
  matrix products  39.7 us (13%)
  blocking collectives  21.5 us (7%)
  between operations  20.6 us (7%)
  local copies, waits for them, and re-layouts  12.4 us (4%)
  starting transfers between devices  4.01 us (1%)
    reduce_scatter x1, waiting for transfers between devices, shards(): lax.psum_scatter(partial_ffn.astype(jnp.bfloat16), 'tp', scatter_dimensio...  38.9 us
    reduce_scatter x1, waiting for transfers between devices, shards(): lax.psum_scatter(partial_rows.astype(jnp.bfloat16), 'tp', scatter_dimensi...  36.8 us
    all_gather x1, waiting for transfers between devices, turned_gather(): out, at, finished = (lax.all_gather(both, axis, axis=0, tiled=True), 0, [])  36.6 us
    all_gather x1, waiting for transfers between devices, shards(): whole_rows = lax.all_gather(normed_own, 'tp', axis=0, tiled=True)  32.7 us
    unnamed x2, blocking collectives  21.5 us
    all_gather x2, waiting for transfers between devices, entering(): lax.all_gather(part.astype(kind), axis)  15.5 us
    dot_general x1, matrix products, shards(): jnp.dot(activated, full_down, preferred_element_type=jnp.float32)  10 us
    dot_general x4, matrix products, advance(): jnp.einsum('thd,hde->the', pieces[0], carry_state.astype(jnp.bfloat16), p...  7.74 us
  transfers between devices with their start and end apart: 7, of which 7 were waited for; matrix products, arithmetic and copies ran while one was open for 5% of the time, Pallas kernels for 0%

commit v1 on v0

--- a/solution.py
+++ b/solution.py
@@ -12,10 +12,15 @@
 tiny_stabilizer = 1e-05
 
 
+def swapped_in(array, axis, dim):
+    stack = jnp.stack([array] * lax.axis_size(axis))
+    return jnp.concatenate(lax.all_to_all(stack, axis, 0, 0), axis=dim)
+
+
 def turned_gather(arrays, axis, dims):
     turned = [jnp.moveaxis(a, dim, 0) for a, dim in zip(arrays, dims)]
     both = jnp.concatenate([t.reshape(len(t), -1) for t in turned], axis=1)
-    out, at, finished = (lax.all_gather(both, axis, axis=0, tiled=True), 0, [])
+    out, at, finished = (swapped_in(both, axis, 0), 0, [])
     for t, dim in zip(turned, dims):
         piece = out[:, at : at + t[0].size].reshape(-1, *t.shape[1:])
         finished.append(jnp.moveaxis(piece, 0, dim))

time: 316 us -> 358 us (1.13)
  local copies, waits for them, and re-layouts: 12.4 us -> 29.1 us
  waiting for transfers between devices: 165 us -> 179 us
  matrix products: 39.7 us -> 45.4 us
  starting transfers between devices: 4.01 us -> 7.95 us
    all_to_all x0 -> x1, waiting for transfers between devices: none -> 92.9 us  [swapped_in(): return jnp.concatenate(lax.all_to_all(stack, axis, 0, 0), axis=dim)]
    all_gather x1 -> x0, waiting for transfers between devices: 36.6 us -> none  [turned_gather(): out, at, finished = (lax.all_gather(both, axis, axis=0, tiled=True), 0, [])]
    all_gather x1, waiting for transfers between devices: 32.7 us -> 0.01 us  [shards(): whole_rows = lax.all_gather(normed_own, 'tp', axis=0, tiled=True)]
    all_to_all x0 -> x1, local copies, waits for them, and re-layouts: none -> 11.7 us  [swapped_in(): return jnp.concatenate(lax.all_to_all(stack, axis, 0, 0), axis=dim)]
    reduce_scatter x1, waiting for transfers between devices: 36.8 us -> 26.5 us  [shards(): lax.psum_scatter(partial_rows.astype(jnp.bfloat16), 'tp', scatter_dimensi...]
    dot_general x1, matrix products: 10 us -> 16.3 us  [shards(): jnp.dot(activated, full_down, preferred_element_type=jnp.float32)]
    all_to_all x0 -> x1, starting transfers between devices: none -> 6.08 us  [swapped_in(): return jnp.concatenate(lax.all_to_all(stack, axis, 0, 0), axis=dim)]
    another operation x4 -> x5, local copies, waits for them, and re-layouts: 0.23 us -> 5.19 us  [the longest x1 4.96 us: swapped_in(): stack = jnp.stack([array] * lax.axis_size(axis))]
  transfers between devices with their start and end apart: 7 -> 7, of which waited for: 7 -> 6; matrix products, arithmetic and copies ran while one was open for 5% -> 9% of each run, Pallas kernels for 0% -> 0%
where the time goes in v1:
time: 358 us; the launch traced here: 356 us
  waiting for transfers between devices  179 us (50%)
  other arithmetic  54.1 us (15%)
  matrix products  45.4 us (13%)
  local copies, waits for them, and re-layouts  29.1 us (8%)
  blocking collectives  21.5 us (6%)
  between operations  19.1 us (5%)
  starting transfers between devices  7.95 us (2%)
    all_to_all x1, waiting for transfers between devices, swapped_in(): return jnp.concatenate(lax.all_to_all(stack, axis, 0, 0), axis=dim)  92.9 us
    reduce_scatter x1, waiting for transfers between devices, shards(): lax.psum_scatter(partial_ffn.astype(jnp.bfloat16), 'tp', scatter_dimensio...  41 us
    reduce_scatter x1, waiting for transfers between devices, shards(): lax.psum_scatter(partial_rows.astype(jnp.bfloat16), 'tp', scatter_dimensi...  26.5 us
    unnamed x2, blocking collectives  21.5 us
    dot_general x1, matrix products, shards(): jnp.dot(activated, full_down, preferred_element_type=jnp.float32)  16.3 us
    all_gather x2, waiting for transfers between devices, entering(): lax.all_gather(part.astype(kind), axis)  15.5 us
    all_to_all x1, local copies, waits for them, and re-layouts, swapped_in(): return jnp.concatenate(lax.all_to_all(stack, axis, 0, 0), axis=dim)  11.7 us
    dot_general x4, matrix products, advance(): jnp.einsum('thd,hde->the', pieces[0], carry_state.astype(jnp.bfloat16), p...  7.76 us
  transfers between devices with their start and end apart: 7, of which 6 were waited for; matrix products, arithmetic and copies ran while one was open for 9% of the time, Pallas kernels for 0%

profile of v1, /device:TPU:0, one launch (start us, length us, event | category | flops | bytes accessed | tf_op | source)
XLA Modules:
  0.0 356.1 jit_solution(813721763161240955)
XLA Ops:
  6.5 2.4 reduce-window.6
  9.5 1.4 bitcast_convert_fusion
  11.0 3.1 fusion.56
  14.8 2.0 convolution_bitcast_fusion.1
  16.9 9.8 %while.24 = (s32[]{:T(128)}, f32[1,256,512]{2,1,0:T(8,128)S(1)}, f32[4,1]{0,1:T(1,128)S(1)}, f32[4,1,256,512]{3,2,1,0:T(8,128)}, s32[]{:T(128)}, /*index=5*/s32[]{:T(128)}) while((s32[]{:T(128)}, f32[1,256,512]{2,1,0:T(8,128)S(1)}, f32[4,1]{0,1:T(1,128)S(1)}, f32[4,1,256,512]{3,2,1,0:T(8,128)}, s32[]{:T(128)}, ...), condition=%wide.region_4.5_spmd.clone, body=%wide.region_3.4_spmd.clone.sunk | while | flops 393219 | bytes 1572971 | solution.py:168
  17.5 1.8 bitcast_add_fusion.8
  19.9 1.8 bitcast_add_fusion.8
  22.4 1.8 bitcast_add_fusion.8
  24.8 1.8 bitcast_add_fusion.8
  28.8 1.4 dynamic-update-slice
  30.2 10.8 %all-reduce = bf16[4]{0:T(256)(128)(2,1)S(1)} all-reduce(bf16[4]{0:T(256)(128)(2,1)S(1)} %dynamic-update-slice), channel_id=1, replica_groups=mesh['sp_0'=4,'sp_1'=4,'tp'=8] {'sp_1'}, use_global_device_ids=true, to_apply=%add | all-reduce | flops 4 | bytes 16
  42.3 11.9 %all-gather.10.cloned.1.call-done = bf16[4,256,512]{2,1,0:T(8,128)(2,1)} async-done(((bf16[1,256,512]{2,1,0:T(8,128)(2,1)}), bf16[4,256,512]{2,1,0:T(8,128)(2,1)}) %all-gather.10.cloned.1.call-update) | async-done | bytes 1048592 | tf_op jit(solution)/shard_map/all_gather | solution.py:43
  54.2 4.0 %fusion.70 = bf16[1,1,256,512]{3,2,1,0:T(8,128)(2,1)} fusion(f32[]{:T(128)} %bitcast.39, f32[]{:T(128)} %bitcast.40, f32[]{:T(128)} %bitcast.41, f32[]{:T(128)} %bitcast.42, bf16[4,256,512]{2,1,0:T(8,128)(2,1)} %all-gather.10.cloned.1.call-done), kind=kLoop, calls=%fused_computation.102 | loop fusion | flops 1572864 | bytes 1310736 | tf_op jit(solution)/shard_map/convert_element_type | solution.py:43
  59.6 1.4 dynamic-update-slice.1
  61.0 10.7 %all-reduce.1 = bf16[4]{0:T(256)(128)(2,1)S(1)} all-reduce(bf16[4]{0:T(256)(128)(2,1)S(1)} %dynamic-update-slice.1), channel_id=2, replica_groups=mesh['sp_0'=4,'sp_1'=4,'tp'=8] {'sp_0'}, use_global_device_ids=true, to_apply=%add.1 | all-reduce | flops 4 | bytes 16
  77.4 1.9 fusion.61
  79.3 3.6 %all-gather.6.cloned.1.call-done = bf16[4,1,256,512]{3,2,1,0:T(8,128)(2,1)} async-done(((bf16[1,1,256,512]{3,2,1,0:T(8,128)(2,1)}), bf16[4,1,256,512]{3,2,1,0:T(8,128)(2,1)}) %all-gather.6.cloned.1.call-update) | async-done | bytes 1048592 | tf_op jit(solution)/shard_map/all_gather | solution.py:43
  83.0 3.9 %fusion.69 = f32[1,256,512]{2,1,0:T(8,128)S(1)} fusion(bf16[4,1,256,512]{3,2,1,0:T(8,128)(2,1)} %all-gather.6.cloned.1.call-done, f32[]{:T(128)} %bitcast.39, f32[]{:T(128)} %bitcast.40, f32[]{:T(128)} %bitcast.41, f32[]{:T(128)} %bitcast.42, f32[]{:T(128)} %bitcast.33, f32[]{:T(128)S(6)} %convert.26, f32[]{:T(128)S(6)} %convert.27, f32[]{:T(128)} %bitcast.38, ...), kind=kLoop, calls=%fused_computation.99 | loop fusion | flops 4194304 | bytes 2621484 | tf_op jit(solution)/shard_map/add | solution.py:121
  86.9 17.8 %while.23 = (s32[]{:T(128)}, f32[1,256,512]{2,1,0:T(8,128)S(1)}, f32[4,256,1,512]{3,1,2,0:T(8,128)}, f32[4,1]{0,1:T(1,128)S(1)}, f32[4,1,256,512]{3,2,1,0:T(8,128)}, /*index=5*/bf16[4,256,1,256]{3,1,2,0:T(8,128)(2,1)}, s32[]{:T(128)}) while((s32[]{:T(128)}, f32[1,256,512]{2,1,0:T(8,128)S(1)}, f32[4,256,1,512]{3,1,2,0:T(8,128)}, ...), condition=%wide.region_6.7_spmd, body=%wide.region_5.6_spmd.sunk | while | flops 67502080 | bytes 2753641 | solution.py:183
  86.9 1.9 fusion.118
  89.4 1.9 bitcast_add_fusion.7
  91.3 1.9 fusion.118
  93.9 1.9 bitcast_add_fusion.7
  95.8 1.9 fusion.118
  98.3 1.9 bitcast_add_fusion.7
  100.2 1.9 fusion.118
  102.8 1.9 bitcast_add_fusion.7
  104.7 4.2 %fusion.102 = (f32[4,256]{1,0:T(4,128)S(1)}, f32[4,256,1,512]{3,1,0,2:T(8,128)}) fusion(f32[4,256,1,512]{3,1,2,0:T(8,128)} %get-tuple-element.60, bf16[4,256,512]{2,1,0:T(8,128)(2,1)} %bitcast.154, bf16[4,256,128]{2,1,0:T(8,128)(2,1)} %bitcast.159, bf16[4,256,128]{2,1,0:T(8,128)(2,1)S(1)} %bitcast.157, f32[4,256]{1,0:T(4,128)S(1)} %get-tuple-element.155, ...), kind=kOutput, calls=%fused_computation.160 | convolution fusion | flops 406846464 | bytes 6889472 | tf_op jit(solution)/shard_map/vmap(htm,mhe->the)/dot_general | solution.py:95
  108.9 2.1 multiply_reduce_fusion
  111.1 2.2 fusion.31
  113.3 4.3 %convolution_convert_fusion.1 = bf16[1024,2048]{1,0:T(8,128)(2,1)} fusion(bf16[1024,512]{1,0:T(8,128)(2,1)S(1)} %fusion.31, bf16[512,2048]{1,0:T(8,128)(2,1)S(1)} %copy-done), kind=kOutput, calls=%fused_computation.14 | convolution fusion | flops 2149580800 | bytes 7340032 | tf_op jit(solution)/shard_map/dot_general | solution.py:195
  118.8 5.0 %stack.2 = bf16[16,128,2112]{1,2,0:T(8,128)(2,1)} broadcast(bf16[128,2112]{0,1:T(8,128)(2,1)S(1)} %pad_maximum_fusion), dimensions={1,2} | broadcast | bytes 9191424 | tf_op jit(solution)/shard_map/stack | solution.py:16
  123.7 6.1 %all-to-all-start = ((bf16[16,128,2112]{1,2,0:T(8,128)(2,1)}), bf16[16,128,2112]{1,2,0:T(8,128)(2,1)}, u32[]{:S(2)}, u32[]{:S(2)}) async-start(bf16[16,128,2112]{1,2,0:T(8,128)(2,1)} %stack.2), calls=%async_computation.1 | async-start | bytes 17301504 | tf_op jit(solution)/shard_map/all_to_all | solution.py:17
  130.0 26.5 %reduce-scatter.3.cloned.1.call-done = bf16[128,2048]{1,0:T(8,128)(2,1)} async-done(((bf16[1024,2048]{1,0:T(8,128)(2,1)}), bf16[128,2048]{1,0:T(8,128)(2,1)}) %reduce-scatter.3.cloned.1.call-update) | async-done | bytes 524304 | tf_op jit(solution)/shard_map/reduce_scatter | solution.py:196
  156.5 1.5 fusion.45
  158.0 1.5 multiply_reduce_fusion.2
  159.5 2.3 add_convert_fusion.1
  162.1 92.9 %all-to-all-done = bf16[16,128,2112]{1,2,0:T(8,128)(2,1)} async-done(((bf16[16,128,2112]{1,2,0:T(8,128)(2,1)}), bf16[16,128,2112]{1,2,0:T(8,128)(2,1)}, u32[]{:S(2)}, u32[]{:S(2)}) %all-to-all-start) | async-done | bytes 8650784 | tf_op jit(solution)/shard_map/all_to_all | solution.py:17
  255.1 11.7 %copy.70 = bf16[16,128,2112]{2,1,0:T(8,128)(2,1)} copy(bf16[16,128,2112]{1,2,0:T(8,128)(2,1)} %all-to-all-done) | data formatting | bytes 17301504 | tf_op jit(solution)/shard_map/all_to_all | solution.py:17
  266.8 7.4 %fusion.35 = bf16[1024,704]{0,1:T(8,128)(2,1)S(1)} fusion(bf16[1024,2048]{1,0:T(8,128)(2,1)} %all-gather.8.cloned.1.call-done, bf16[2048,2112]{1,0:T(8,128)(2,1)} %bitcast.147), kind=kOutput, calls=%fused_computation.53 | convolution fusion | flops 2953510912 | bytes 8781824 | tf_op jit(solution)/shard_map/dot_general | solution.py:207
  274.4 3.3 fusion.32
  278.0 1.5 collective-permute-start
  279.5 2.7 collective-permute-done
  282.4 2.5 maximum_convert_fusion.1
  284.9 2.5 maximum_convert_fusion
  287.4 16.3 %convolution_convert_fusion = bf16[1024,2048]{1,0:T(8,128)(2,1)} fusion(bf16[2048,2112]{1,0:T(8,128)(2,1)S(1)} %bitcast.149, f32[1026,704]{0,1:T(8,128)} %maximum_convert_fusion.1, f32[1026,704]{0,1:T(8,128)} %maximum_convert_fusion, f32[704]{0:T(1024)S(1)} %get-tuple-element.130, f32[704]{0:T(1024)S(1)} %get-tuple-element.131, ...), kind=kOutput, calls=%fused_computation.13 | convolution fusion | flops 2970746880 | bytes 24674304 | tf_op jit(solution)/shard_map/dot_general | solution.py:216
  303.7 41.0 %reduce-scatter.5.cloned.1.call-done = bf16[128,2048]{1,0:T(8,128)(2,1)} async-done(((bf16[1024,2048]{1,0:T(8,128)(2,1)}), bf16[128,2048]{1,0:T(8,128)(2,1)}) %reduce-scatter.5.cloned.1.call-update) | async-done | bytes 524304 | tf_op jit(solution)/shard_map/reduce_scatter | solution.py:217
  347.4 2.2 add_convert_fusion
  (96 shorter events, 15.8 us)
Async XLA Ops:
  6.5 106.8 %copy-start = (bf16[512,2048]{1,0:T(8,128)(2,1)S(1)}, bf16[512,2048]{1,0:T(8,128)(2,1)}, u32[]{:S(2)}) copy-start(bf16[512,2048]{1,0:T(8,128)(2,1)} %param.24) | copy-start | bytes 6291460
  6.5 47.6 %all-gather.10.cloned.1.call-start = ((), (), s32[]{:S(2)}) async-start(), calls=%async_computation.7 | async-start | bytes 1310720 | tf_op jit(solution)/shard_map/all_gather | solution.py:43
  9.5 5.3 %copy-start.6 = (bf16[1024,512]{1,0:T(8,128)(2,1)S(1)}, bf16[1024,512]{1,0:T(8,128)(2,1)}, u32[]{:S(2)}) copy-start(bf16[1024,512]{1,0:T(8,128)(2,1)} %param.20) | copy-start | bytes 3145732
  14.0 0.8 copy-start.5
  16.9 10.6 %copy-start.16 = (u32[128]{0:T(128)S(1)}, u32[128]{0:T(128)}, u32[]{:S(2)}) copy-start(u32[128]{0:T(128)} %constant.99) | copy-start | bytes 1540
  16.9 41.3 %copy-start.15 = (u32[128]{0:T(128)S(1)}, u32[128]{0:T(128)}, u32[]{:S(2)}) copy-start(u32[128]{0:T(128)} %constant.104) | copy-start | bytes 1540
  27.4 55.6 %all-gather.6.cloned.1.call-start = ((), (), s32[]{:S(2)}) async-start(), calls=%async_computation.3 | async-start | bytes 1310720 | tf_op jit(solution)/shard_map/all_gather | solution.py:43
  58.2 98.3 %reduce-scatter.3.cloned.1.call-start = ((), (), s32[]{:S(2)}) async-start(), calls=%async_computation.4 | async-start | bytes 4718592 | tf_op jit(solution)/shard_map/reduce_scatter | solution.py:196
  108.9 2.2 copy-start.2
  117.6 0.9 copy-start.7
  117.6 1.0 copy-start.8
  117.6 1.1 copy-start.9
  123.7 6.2 %copy-start.11 = (f32[2,2048]{1,0:T(2,128)S(1)}, f32[2,2048]{1,0:T(2,128)}, u32[]{:S(2)}) copy-start(f32[2,2048]{1,0:T(2,128)} %param.26) | copy-start | bytes 49156
  123.7 6.2 %copy-start.12 = (f32[2,2048]{1,0:T(2,128)S(1)}, f32[2,2048]{1,0:T(2,128)}, u32[]{:S(2)}) copy-start(f32[2,2048]{1,0:T(2,128)} %param.25) | copy-start | bytes 49156
  123.7 131.3 %all-to-all-start = ((bf16[16,128,2112]{1,2,0:T(8,128)(2,1)}), bf16[16,128,2112]{1,2,0:T(8,128)(2,1)}, u32[]{:S(2)}, u32[]{:S(2)}) async-start(bf16[16,128,2112]{1,2,0:T(8,128)(2,1)} %stack.2), calls=%async_computation.1 | async-start | bytes 17301504 | tf_op jit(solution)/shard_map/all_to_all | solution.py:17
  129.8 32.2 %copy-start.10 = (f32[2,3,704]{2,0,1:T(2,128)S(1)}, f32[2,3,704]{2,0,1:T(2,128)}, u32[]{:S(2)}) copy-start(f32[2,3,704]{2,0,1:T(2,128)} %param.29) | copy-start | bytes 50692
  129.8 136.9 %all-gather.8.cloned.1.call-start = ((), (), s32[]{:S(2)}) async-start(), calls=%async_computation.5 | async-start | bytes 4718592 | tf_op jit(solution)/shard_map/all_gather | solution.py:205
  161.8 182.9 %reduce-scatter.5.cloned.1.call-start = ((), (), s32[]{:S(2)}) async-start(), calls=%async_computation.6 | async-start | bytes 4718592 | tf_op jit(solution)/shard_map/reduce_scatter | solution.py:217
  266.8 7.6 %copy-start.4 = (bf16[16,128,2112]{2,1,0:T(8,128)(2,1)S(1)}, bf16[16,128,2112]{2,1,0:T(8,128)(2,1)}, u32[]{:S(2)}) copy-start(bf16[16,128,2112]{2,1,0:T(8,128)(2,1)} %copy.70) | copy-start | bytes 25952260
  266.8 7.6 %copy-start.14 = (bf16[1024,2048]{1,0:T(8,128)(2,1)S(1)}, bf16[1024,2048]{1,0:T(8,128)(2,1)}, u32[]{:S(2)}) copy-start(bf16[1024,2048]{1,0:T(8,128)(2,1)} %all-gather.8.cloned.1.call-done) | copy-start | bytes 12582916
  274.4 5.2 %copy-start.13 = (f32[2,704]{1,0:T(2,128)S(1)}, f32[2,704]{1,0:T(2,128)}, u32[]{:S(2)}) copy-start(f32[2,704]{1,0:T(2,128)} %param.30) | copy-start | bytes 16900
  278.0 4.3 %collective-permute-start = (bf16[4,704]{0,1:T(8,128)(2,1)S(1)}, bf16[4,704]{0,1:T(8,128)(2,1)S(1)}, u32[]{:S(2)}, u32[]{:S(2)}) collective-permute-start(bf16[4,704]{0,1:T(8,128)(2,1)S(1)} %pad_maximum_fusion.1), channel_id=1, source_target_pairs={{0,8},{8,16},{16,24},{24,32},{32,40},{40,48},{48,56},{56,64},{64,7... | collective-permute-start | bytes 16904 | tf_op jit(solution)/shard_map/ppermute | solution.py:61
  303.7 41.1 %copy-start.3 = (bf16[128,2048]{1,0:T(8,128)(2,1)S(1)}, bf16[128,2048]{1,0:T(8,128)(2,1)}, u32[]{:S(2)}) copy-start(bf16[128,2048]{1,0:T(8,128)(2,1)} %add_convert_fusion.1) | copy-start | bytes 1572868
  303.7 45.9 %copy-start.1 = (bf16[512,2048]{1,0:T(8,128)(2,1)S(1)}, bf16[512,2048]{1,0:T(8,128)(2,1)}, u32[]{:S(2)}) copy-start(bf16[512,2048]{1,0:T(8,128)(2,1)} %param.24) | copy-start | bytes 6291460
Sparse Core Ops, SparseCore 0:
  27.5 26.5 all-gather.9
  58.3 24.6 all-gather.5
  117.8 38.6 reduce-scatter.2
  162.0 31.2 all-gather.7
  303.8 40.8 reduce-scatter.4
